TPU v7x, 32 devices: a whole 2x2x4 slice. The times are simulated.
32 devices in a mesh: fs: 8 (over z, x), tp: 4 (over y, core).
Axes of the slice: x: 2, y: 2, z: 4, core: 2. Of those that a mesh axis runs over, the one named last changes fastest.
Arguments:
- tokens: bfloat16 [4096, 2048], P('fs', 'tp'), may hold values from -6 to 6
- pre_gain: float32 [2048], P('fs'), may hold values from 0.1 to 1.9
- gate_weight: float32 [2048, 6144], P('fs', 'tp'), may hold values from -0.125 to 0.125
- up_weight: float32 [2048, 6144], P('fs', 'tp'), may hold values from -0.125 to 0.125
- down_weight: float32 [2048, 6144], P('fs', 'tp'), may hold values from -0.078125 to 0.078125
- post_gain: float32 [2048], P('tp'), may hold values from 0.1 to 1.9
Outputs:
- result: bfloat16 [4096, 2048], P('fs', 'tp')
- gate_ready: bfloat16 [2048, 6144], P(None, 'tp')
- up_ready: bfloat16 [2048, 6144], P(None, 'tp')
- down_ready: bfloat16 [2048, 6144], P(None, 'tp')
All inputs are finite; a program needn't handle non-finite values.
Results may differ from a plain program's by a relative error of at most 0.015.
Values may be sent and summed in bfloat16 or wider, within the bound.
A program may use at most 128 MiB of HBM per device.

v0:
```python
import functools

import jax
import jax.numpy as jnp
from jax import lax
from jax.experimental import pallas as pl
from jax.experimental.pallas import tpu as pltpu
from jax.sharding import PartitionSpec as P

EPS = 1e-06
MESH = pl.DeviceIdType.MESH
P_PART, Q_PART = 0, 1
UP, DOWN, RIGHT, LEFT = 0, 1, 2, 3
CHUNKS = 4


def kernel(
    fs, tp, lines, cols,
    tokens, pre_gain, gate_weight, up_weight, down_weight,
    gate, squares, squares_in, gate_out, up_out, down_out,
    staged, gains_in, whole, normed, hidden, part, parts_in,
    send_sem, recv_sem, stage_sem, tok_send, tok_recv, tok_own,
    rs_send, rs_recv, sq_send, sq_recv,
):
    weights, outs = (gate_weight, up_weight, down_weight), (gate_out, up_out, down_out)
    depth, width = gate_weight.shape
    half = depth // 2
    rows, block = tokens.shape
    me_fs, me = lax.axis_index("fs"), lax.axis_index("tp")
    z, x = me_fs // cols, lax.rem(me_fs, cols)
    finals = []

    sides = {
        UP: (z < lines - 1, me_fs + cols),
        DOWN: (z > 0, me_fs - cols),
        RIGHT: (x < cols - 1, me_fs + 1),
        LEFT: (x > 0, me_fs - 1),
    }
    peers = [lax.rem(me + j, tp) for j in range(1, tp)]

    def piece(m, which, shard):
        if m < 2:
            return outs[m].at[pl.ds(pl.multiple_of(shard * depth, 16), depth), :]
        return outs[2].at[pl.ds(pl.multiple_of(shard * depth + which * half, 16), half), :]

    def describe(m, which, shard, side, target):
        ref = piece(m, which, shard)
        return pltpu.make_async_remote_copy(
            src_ref=ref, dst_ref=ref,
            send_sem=send_sem.at[m, which, shard, side],
            recv_sem=recv_sem.at[m, which, shard],
            device_id={"fs": target, "tp": me}, device_id_type=MESH,
        )

    def send(m, which, shard, side, extra=None):
        there, target = sides[side]
        cond = there if extra is None else jnp.logical_and(there, extra)

        @pl.when(cond)
        def _():
            describe(m, which, shard, side, target).start()

        def finish():
            @pl.when(cond)
            def _():
                describe(m, which, shard, side, target).wait_send()

        finals.append(finish)

    def arrive(m, which, shard, cond):
        @pl.when(cond)
        def _():
            describe(m, which, shard, 0, lax.rem(me_fs + 1, fs)).wait_recv()

    barrier = pltpu.get_barrier_semaphore()
    for side in sides:
        there, target = sides[side]

        @pl.when(there)
        def _():
            pl.semaphore_signal(barrier, inc=1, device_id={"fs": target, "tp": me}, device_id_type=MESH)

    for peer in peers:
        pl.semaphore_signal(barrier, inc=1, device_id={"fs": me_fs, "tp": peer}, device_id_type=MESH)

    stages = [pltpu.make_async_copy(weights[m], staged.at[m], stage_sem.at[m]) for m in range(3)]
    for c in stages:
        c.start()
    own_tokens = pltpu.make_async_copy(tokens, whole.at[me], tok_own)
    own_tokens.start()
    gains_in[...] = jnp.transpose(jnp.broadcast_to(pre_gain[0:1, :], (128, depth)))

    def cast(m):
        stages[m].wait()

        @pl.loop(0, depth // 16)
        def _(i):
            here = pl.ds(pl.multiple_of(i * 16, 16), 16)
            v = staged[m, here, :]
            if m < 2:
                v = gains_in[here, 0:1] * v
            outs[m][pl.ds(pl.multiple_of(me_fs * depth + i * 16, 16), 16), :] = v.astype(jnp.bfloat16)

    def token_copy(j):
        return pltpu.make_async_remote_copy(
            src_ref=tokens, dst_ref=whole.at[me], send_sem=tok_send.at[j], recv_sem=tok_recv.at[j],
            device_id={"fs": me_fs, "tp": peers[j]}, device_id_type=MESH,
        )

    def start_own(m, which_sides=(UP, DOWN, RIGHT, LEFT)):
        for side in which_sides:
            send(m, Q_PART, me_fs, side)

    cast(0)
    pl.semaphore_wait(barrier, tp - 1 + sum(there.astype(jnp.int32) for there, _ in sides.values()))
    start_own(0)
    for j in range(tp - 1):
        token_copy(j).start()
    cast(1)
    cast(2)

    def normalize():
        own_tokens.wait()
        for j in range(tp - 1):
            token_copy(j).wait_recv()
        step = 64

        @pl.loop(0, rows // step)
        def _(i):
            here = pl.ds(pl.multiple_of(i * step, step), step)
            total = jnp.zeros((step, 1), jnp.float32)
            for t in range(tp):
                v = whole[t, here, :].astype(jnp.float32)
                total = total + jnp.sum(v * v, axis=1, keepdims=True)
            scale = lax.rsqrt(total / (tp * block) + EPS)
            for t in range(tp):
                v = whole[t, here, :].astype(jnp.float32)
                normed[here, t * block:(t + 1) * block] = (v * scale).astype(jnp.bfloat16)

    def along_x(m, which, line, cond=None):
        for r in range(cols - 1):
            for side, column in ((RIGHT, x - 1 - r), (LEFT, x + 1 + r)):
                there = jnp.logical_and(column >= 0, column < cols)
                if cond is not None:
                    there = jnp.logical_and(there, cond)
                arrive(m, which, line * cols + column, there)
                if r < cols - 2:
                    send(m, which, line * cols + column, side, there)

    def valid(line):
        return jnp.logical_and(line >= 0, line < lines)

    def along_z(m, which, s, columns, cond=None):
        for side, line in ((UP, z - 1 - s), (DOWN, z + 1 + s)):
            there = valid(line) if cond is None else jnp.logical_and(valid(line), cond)
            for column in columns:
                shard = line * cols + column
                arrive(m, which, shard, there)
                if s < lines - 2:
                    send(m, which, shard, side, there)
                if which == Q_PART:
                    send(m, which, shard, RIGHT, there)
                    send(m, which, shard, LEFT, there)

    tile = 256

    def project(m):
        along_x(m, Q_PART, z)
        for s in range(lines - 1):
            for line in (z - 1 - s, z + 1 + s):
                along_x(m, Q_PART, line, valid(line))

        @pl.loop(0, width // tile)
        def _(i):
            here = pl.ds(pl.multiple_of(i * tile, tile), tile)
            product = jnp.dot(normed[...], outs[m][:, here], preferred_element_type=jnp.float32)
            if m == 0:
                gate[:, here] = product
            else:
                g = gate[:, here]
                hidden[:, here] = (g / (1.0 + jnp.exp(-g)) * product).astype(jnp.bfloat16)

    early = max(0, lines - 3)
    for s in range(lines - 1):
        along_z(0, Q_PART, s, [x])
        if s == early:
            start_own(1)
            for side in (RIGHT, LEFT):
                send(2, P_PART, me_fs, side)
    normalize()
    for s in range(lines - 1):
        along_z(1, Q_PART, s, [x])
        if s == early:
            start_own(2, (UP, DOWN))
            along_x(2, P_PART, z)
            for column in range(cols):
                for side in (UP, DOWN):
                    send(2, P_PART, z * cols + column, side)
            project(0)
    start_own(2, (RIGHT, LEFT))

    def share_copy(line, sender, column, which):
        return pltpu.make_async_remote_copy(
            src_ref=part.at[line, column, which], dst_ref=parts_in.at[sender, column, which],
            send_sem=rs_send.at[line, column, which], recv_sem=rs_recv.at[sender, column, which],
            device_id={"fs": me_fs, "tp": line}, device_id_type=MESH,
        )

    def mix(line, column, which):
        here = pl.ds(pl.multiple_of((line * cols + column) * depth + which * half, 16), half)
        product = lax.dot_general(
            hidden[...], outs[2][here, :], (((1,), (1,)), ((), ())), preferred_element_type=jnp.float32
        )
        part[line, column, which] = product.astype(jnp.bfloat16)

        @pl.when(line != me)
        def _():
            share_copy(line, me, column, which).start()

    def mix_both(s, column, which):
        @pl.loop(0, 2)
        def _(i):
            line = z + (1 + s) * (2 * i - 1)

            @pl.when(valid(line))
            def _():
                mix(line, column, which)

    def others(action):
        for j in range(1, cols):
            action(lax.rem(x + j, cols))

    def near(s):
        mix_both(s, x, Q_PART)

        @pl.loop(0, cols)
        def _(c):
            mix_both(s, lax.rem(x + c, cols), P_PART)

    def far(s):
        for line in (z - 1 - s, z + 1 + s):
            along_x(2, Q_PART, line, valid(line))
        others(lambda column: mix_both(s, column, Q_PART))

    inner = jnp.logical_and(z > 0, z < lines - 1)

    def down_step(s, cond=None):
        along_z(2, Q_PART, s, [x], cond)
        along_z(2, P_PART, s, range(cols), cond)

    down_step(0)
    for s in range(1, lines - 2):
        down_step(s, inner)
    project(1)
    mix(z, x, Q_PART)

    @pl.loop(0, cols)
    def _(c):
        mix(z, lax.rem(x + c, cols), P_PART)

    if lines > 2:
        near(0)
    for s in range(1, lines - 2):
        down_step(s, jnp.logical_not(inner))
        if s == 1:
            along_x(2, Q_PART, z)
            others(lambda column: mix(z, column, Q_PART))
        near(s)
        far(s - 1)
    last = lines - 2
    if last > 0:
        along_z(2, Q_PART, last, [x])
        mix_both(last, x, Q_PART)
    else:
        mix_both(last, x, Q_PART)
    if last < 2:
        along_x(2, Q_PART, z)
        others(lambda column: mix(z, column, Q_PART))
    if last > 0:
        far(last - 1)
    for column in range(cols):
        if last > 0:
            along_z(2, P_PART, last, [column])
        mix_both(last, column, P_PART)
    far(last)

    for peer in peers:
        for column in range(cols):
            for which in range(2):
                share_copy(peer, peer, column, which).wait_recv()
    step = 128

    @pl.loop(0, rows // step)
    def _(i):
        here = pl.ds(pl.multiple_of(i * step, step), step)
        square = jnp.zeros((step, 1), jnp.float32)
        for column in range(cols):
            for which in range(2):
                start = column * depth + which * half
                total = part[me, column, which, here, :].astype(jnp.float32)
                for peer in peers:
                    total = total + parts_in[peer, column, which, here, :].astype(jnp.float32)
                gate[here, start:start + half] = total
                square = square + jnp.sum(total * total, axis=1, keepdims=True)
        squares[:, here] = jnp.transpose(jnp.broadcast_to(square, (step, 128)))[0:8, :]

    def square_copy(j):
        return pltpu.make_async_remote_copy(
            src_ref=squares, dst_ref=squares_in.at[j], send_sem=sq_send.at[j], recv_sem=sq_recv.at[j],
            device_id={"fs": me_fs, "tp": peers[j]}, device_id_type=MESH,
        )

    for j in range(tp - 1):
        square_copy(j).start()
    for finish in finals:
        finish()
    for j in range(tp - 1):
        token_copy(j).wait_send()
        for column in range(cols):
            for which in range(2):
                share_copy(peers[j], me, column, which).wait_send()
    for j in range(tp - 1):
        square_copy(j).wait_recv()
    for j in range(tp - 1):
        square_copy(j).wait_send()


def write_out(
    width, share, squares, squares_in, gate_held, up_held, down_held, post_gain,
    result_out, gate_out, up_out, down_out, result, sems, last,
):
    copies = []
    for k, (ref, out) in enumerate(((gate_held, gate_out), (up_held, up_out), (down_held, down_out))):
        size = ref.shape[0] // CHUNKS
        for c in range(CHUNKS):
            here = pl.ds(c * size, size)
            copies.append(pltpu.make_async_copy(ref.at[here, :], out.at[here, :], sems.at[k, c]))
    for c in copies:
        c.start()
    rows, block = result.shape
    gains = post_gain[0:1, :]
    step = 128

    @pl.loop(0, rows // step)
    def _(i):
        here = pl.ds(pl.multiple_of(i * step, step), step)
        total = squares[:, here]
        for j in range(squares_in.shape[0]):
            total = total + squares_in[j, :, here]
        total = jnp.broadcast_to(total[0:1, :], (128, step))
        scale = lax.rsqrt(jnp.transpose(total)[:, 0:1] / width + EPS)
        result[here, :] = (share[here, 0:block] * scale * gains).astype(jnp.bfloat16)

    final = pltpu.make_async_copy(result, result_out, last)
    final.start()
    for c in copies:
        c.wait()
    final.wait()


def solution(mesh):
    fs, tp = mesh.shape["fs"], mesh.shape["tp"]
    lines, cols = tp, fs // tp

    def shards(tokens, pre_gain, gate_weight, up_weight, down_weight, post_gain):
        depth, width = gate_weight.shape
        rows, block = tokens.shape
        hbm = pl.BlockSpec(memory_space=pltpu.HBM)
        vmem = pl.BlockSpec(memory_space=pltpu.VMEM)
        dma = pltpu.SemaphoreType.DMA
        half = depth // 2
        shapes = [(rows, block)] + [(fs * depth, width)] * 3
        held = pl.pallas_call(
            functools.partial(kernel, fs, tp, lines, cols),
            out_shape=(
                pltpu.VMEM((rows, max(width, block)), jnp.float32),
                pltpu.VMEM((8, rows), jnp.float32),
                pltpu.VMEM((tp - 1, 8, rows), jnp.float32),
            ) + tuple(pltpu.VMEM(s, jnp.bfloat16) for s in shapes[1:]),
            in_specs=[hbm, vmem, hbm, hbm, hbm],
            out_specs=(vmem,) * 6,
            scratch_shapes=[
                pltpu.VMEM((3, depth, width), jnp.float32),
                pltpu.VMEM((depth, 128), jnp.float32),
                pltpu.VMEM((tp, rows, block), jnp.bfloat16),
                pltpu.VMEM((rows, tp * block), jnp.bfloat16),
                pltpu.VMEM((rows, width), jnp.bfloat16),
                pltpu.VMEM((tp, cols, 2, rows, half), jnp.bfloat16),
                pltpu.VMEM((tp, cols, 2, rows, half), jnp.bfloat16),
                dma((3, 2, fs, 4)), dma((3, 2, fs)), dma((3,)),
                dma((tp - 1,)), dma((tp - 1,)), dma,
                dma((tp, cols, 2)), dma((tp, cols, 2)), dma((tp - 1,)), dma((tp - 1,)),
            ],
            compiler_params=pltpu.CompilerParams(collective_id=0, has_side_effects=True, vmem_limit_bytes=38 * 1024 * 1024),
        )(tokens, pre_gain[None, :], gate_weight, up_weight, down_weight)
        return tuple(pl.pallas_call(
            functools.partial(write_out, tp * block),
            out_shape=tuple(jax.ShapeDtypeStruct(s, jnp.bfloat16) for s in shapes),
            in_specs=[vmem] * 7,
            out_specs=(hbm,) * 4,
            scratch_shapes=[pltpu.VMEM((rows, block), jnp.bfloat16), dma((3, CHUNKS)), dma],
            compiler_params=pltpu.CompilerParams(vmem_limit_bytes=2 * 1024 * 1024),
        )(*held, post_gain[None, :]))

    return jax.shard_map(
        shards,
        mesh=mesh,
        in_specs=(P("fs", "tp"), P("fs"), P("fs", "tp"), P("fs", "tp"), P("fs", "tp"), P("tp")),
        out_specs=(P("fs", "tp"), P(None, "tp"), P(None, "tp"), P(None, "tp")),
        check_vma=False,
    )
```

profile of v0, /device:TPU:0, one launch (start us, length us, event | category | flops | bytes accessed | tf_op | source)
XLA Modules:
  0.0 206.0 jit_solution(15746758589593282276)
XLA Ops:
  0.6 197.9 %shard_map.93 = (f32[512,1536]{1,0:T(8,128)S(1)}, f32[8,512]{1,0:T(8,128)S(1)}, f32[3,8,512]{2,1,0:T(8,128)S(1)}, bf16[2048,1536]{1,0:T(8,128)(2,1)S(1)}, bf16[2...) custom-call(bf16[512,512]{1,0:T(8,128)(2,1)} %tokens.1, f32[1,256]{1,0:T(1,128)} %bitcast.3, ...), custom_call_target="tpu_custom_call" | custom-call | tf_op jit(solution)/shard_map/pallas_call | solution.py:373
  198.6 0.0 copy-start
  198.6 0.7 copy-done
  199.3 6.7 %shard_map.94 = (bf16[512,512]{1,0:T(8,128)(2,1)}, bf16[2048,1536]{1,0:T(8,128)(2,1)}, bf16[2048,1536]{1,0:T(8,128)(2,1)}, bf16[2048,1536]{1,0:T(8,128)(2,1)}) custom-call(f32[512,1536]{1,0:T(8,128)S(1)} %get-tuple-element.10.share, f32[8,512]{1,0:T(8,128)S(1)} %get-tuple-element.11.squares, f32[3,8,512]{2,1,0:T(8,128)S(1)} %get-tuple-element.12.squares_in, ...), custom_call_target="tpu_custom_call" | custom-call | tf_op jit(solution)/shard_map/pallas_call | solution.py:396
Async XLA Ops:
  198.6 0.7 copy-start
where the time goes:
time: 206 us
  Pallas kernels  205 us (100%)
    pallas_call x1, Pallas kernels, shards(): pl.pallas_call(functools.partial(kernel, fs, tp, lines, cols), out_shape=...  198 us
    pallas_call x1, Pallas kernels, shards(): pl.pallas_call(functools.partial(write_out, tp * block), out_shape=tuple(...  6.71 us

commit v1 on v0

v1 whole, which is shorter than its diff:
```python
import functools

import jax
import jax.numpy as jnp
from jax import lax
from jax.experimental import pallas as pl
from jax.experimental.pallas import tpu as pltpu
from jax.sharding import PartitionSpec as P

EPS = 1e-06
MESH = pl.DeviceIdType.MESH
P_PART, Q_PART = 0, 1
UP, DOWN, RIGHT, LEFT = 0, 1, 2, 3
CHUNKS = 4


def kernel(
    fs, tp, lines, cols,
    tokens, pre_gain, gate_weight, up_weight, down_weight, post_gain,
    totals, squares, squares_in, gains_out, gate_out, up_out, down_out,
    staged, gains_row, gains_in, whole, normed, gate, hidden, part, parts_in, powers,
    send_sem, recv_sem, down_recv, stage_sem, gain_sem, tok_send, tok_recv, tok_own,
    rs_send, rs_recv, sq_send, sq_recv,
):
    weights, outs = (gate_weight, up_weight, down_weight), (gate_out, up_out, down_out)
    depth, width = gate_weight.shape
    half = depth // 2
    rows, block = tokens.shape
    me_fs, me = lax.axis_index("fs"), lax.axis_index("tp")
    z, x = me_fs // cols, lax.rem(me_fs, cols)

    sides = {
        UP: (z < lines - 1, me_fs + cols),
        DOWN: (z > 0, me_fs - cols),
        RIGHT: (x < cols - 1, me_fs + 1),
        LEFT: (x > 0, me_fs - 1),
    }
    peers = [lax.rem(me + j, tp) for j in range(1, tp)]
    corner = jnp.logical_or(z == 0, z == lines - 1)

    def describe(m, which, shard, side, target):
        if m < 2:
            ref = outs[m].at[pl.ds(pl.multiple_of(shard * depth, 16), depth), :]
            landed = recv_sem.at[m, shard]
        else:
            ref = outs[2].at[pl.ds(pl.multiple_of(shard * depth + which * half, 16), half), :]
            landed = down_recv.at[which, shard]
        return pltpu.make_async_remote_copy(
            src_ref=ref, dst_ref=ref, send_sem=send_sem.at[m, side], recv_sem=landed,
            device_id={"fs": target, "tp": me}, device_id_type=MESH,
        )

    def send(m, which, shard, side, extra=None):
        there, target = sides[side]
        cond = there if extra is None else jnp.logical_and(there, extra)

        @pl.when(cond)
        def _():
            describe(m, which, shard, side, target).start()

    def arrive(m, which, shard, cond):
        @pl.when(cond)
        def _():
            describe(m, which, shard, 0, lax.rem(me_fs + 1, fs)).wait_recv()

    def sent(m, side, rows_sent):
        ref = outs[m].at[0:rows_sent, :]
        pltpu.make_async_remote_copy(
            src_ref=ref, dst_ref=ref, send_sem=send_sem.at[m, side], recv_sem=recv_sem.at[0, 0],
            device_id={"fs": lax.rem(me_fs + 1, fs), "tp": me}, device_id_type=MESH,
        ).wait_send()

    barrier = pltpu.get_barrier_semaphore()
    for side in sides:
        there, target = sides[side]

        @pl.when(there)
        def _():
            pl.semaphore_signal(barrier, inc=1, device_id={"fs": target, "tp": me}, device_id_type=MESH)

    for peer in peers:
        pl.semaphore_signal(barrier, inc=1, device_id={"fs": me_fs, "tp": peer}, device_id_type=MESH)

    gain_load = pltpu.make_async_copy(pre_gain, gains_row, gain_sem.at[0])
    gain_load.start()
    size = depth // CHUNKS
    for m in range(3):
        for c in range(CHUNKS):
            here = pl.ds(c * size, size)
            pltpu.make_async_copy(weights[m].at[here, :], staged.at[m, here, :], stage_sem.at[m]).start()
    own_tokens = pltpu.make_async_copy(tokens, whole.at[me], tok_own)
    own_tokens.start()
    post_load = pltpu.make_async_copy(post_gain, gains_out, gain_sem.at[1])
    post_load.start()
    gain_load.wait()
    gains_in[...] = jnp.transpose(jnp.broadcast_to(gains_row[0:1, :], (128, depth)))

    def cast(m):
        pltpu.make_async_copy(weights[m], staged.at[m], stage_sem.at[m]).wait()

        @pl.loop(0, depth // 16)
        def _(i):
            here = pl.ds(pl.multiple_of(i * 16, 16), 16)
            v = staged[m, here, :]
            if m < 2:
                v = gains_in[here, 0:1] * v
            outs[m][pl.ds(pl.multiple_of(me_fs * depth + i * 16, 16), 16), :] = v.astype(jnp.bfloat16)

    def token_copy(j):
        return pltpu.make_async_remote_copy(
            src_ref=tokens, dst_ref=whole.at[me], send_sem=tok_send, recv_sem=tok_recv,
            device_id={"fs": me_fs, "tp": peers[j]}, device_id_type=MESH,
        )

    def token_all():
        ref = whole.at[0:tp - 1]
        return pltpu.make_async_remote_copy(
            src_ref=ref, dst_ref=ref, send_sem=tok_send, recv_sem=tok_recv,
            device_id={"fs": me_fs, "tp": peers[0]}, device_id_type=MESH,
        )

    cast(0)
    pl.semaphore_wait(barrier, tp - 1 + sum(there.astype(jnp.int32) for there, _ in sides.values()))
    for side in sides:
        send(0, Q_PART, me_fs, side)
    for j in range(tp - 1):
        token_copy(j).start()
    cast(1)
    for side in sides:
        send(1, Q_PART, me_fs, side)
    cast(2)
    for side in (RIGHT, LEFT):
        send(2, P_PART, me_fs, side)

    def normalize():
        own_tokens.wait()
        token_all().wait_recv()
        step = 64

        @pl.loop(0, rows // step)
        def _(i):
            here = pl.ds(pl.multiple_of(i * step, step), step)
            total = jnp.zeros((step, 1), jnp.float32)
            for t in range(tp):
                v = whole[t, here, :].astype(jnp.float32)
                total = total + jnp.sum(v * v, axis=1, keepdims=True)
            scale = lax.rsqrt(total / (tp * block) + EPS)
            for t in range(tp):
                v = whole[t, here, :].astype(jnp.float32)
                normed[here, t * block:(t + 1) * block] = (v * scale).astype(jnp.bfloat16)

    def valid(line):
        return jnp.logical_and(line >= 0, line < lines)

    def around(s):
        return (UP, z - 1 - s), (DOWN, z + 1 + s)

    def along_x(m, which, line, cond=None):
        for r in range(cols - 1):
            for side, column in ((RIGHT, x - 1 - r), (LEFT, x + 1 + r)):
                there = jnp.logical_and(column >= 0, column < cols)
                if cond is not None:
                    there = jnp.logical_and(there, cond)
                arrive(m, which, line * cols + column, there)
                if r < cols - 2:
                    send(m, which, line * cols + column, side, there)

    def along_z(m, s):
        for side, line in around(s):
            there = valid(line)
            shard = line * cols + x
            arrive(m, Q_PART, shard, there)
            if s < lines - 2:
                send(m, Q_PART, shard, side, there)
            if m < 2:
                send(m, Q_PART, shard, RIGHT, there)
                send(m, Q_PART, shard, LEFT, there)

    final = {UP: jnp.minimum(me, lines - 2), DOWN: jnp.maximum(me, 1)}
    next_to_end = {UP: z == lines - 2, DOWN: z == 1}

    def put_off(side, line):
        return jnp.logical_and(next_to_end[side], line == final[side])

    def own_down(s):
        for side, behind in ((UP, z), (DOWN, lines - 1 - z)):
            now = behind <= 1 if s == 0 else behind == s + 1
            send(2, Q_PART, me_fs, side, now)
            now = jnp.logical_and(now, jnp.logical_not(put_off(side, z)))
            for c in range(cols):
                send(2, P_PART, z * cols + lax.rem(x + c, cols), side, now)

    def pass_p(s):
        for side, line in around(s):
            there = jnp.logical_and(valid(line), sides[side][0])
            on = jnp.logical_not(put_off(side, line))
            for c in range(cols):
                shard = line * cols + lax.rem(x + c, cols)
                arrive(2, P_PART, shard, there)
                send(2, P_PART, shard, side, jnp.logical_and(there, on))

    for s in range(lines - 1):
        for m in range(2):
            along_z(m, s)
        if s == 0:
            along_x(2, P_PART, z)
        own_down(s)
        if s == 0:
            normalize()
    for s in range(lines - 1):
        along_z(2, s)

    def in_turn(i):
        return me if i is None else jnp.where(i < me, i, i + 1)

    for i in list(range(lines - 1)) + [None]:
        for side in (RIGHT, LEFT):
            send(2, Q_PART, in_turn(i) * cols + x, side)
    for s in range(lines - 2):
        pass_p(s)
    for side in (UP, DOWN):
        for c in range(cols):
            send(2, P_PART, final[side] * cols + lax.rem(x + c, cols), side, next_to_end[side])

    tile = 256

    def project(m):
        along_x(m, Q_PART, z)
        for s in range(lines - 1):
            for _, line in around(s):
                along_x(m, Q_PART, line, valid(line))

        @pl.loop(0, width // tile)
        def _(i):
            here = pl.ds(pl.multiple_of(i * tile, tile), tile)
            product = jnp.dot(normed[...], outs[m][:, here], preferred_element_type=jnp.float32)
            if m == 0:
                gate[:, here] = product
            else:
                g = gate[:, here]
                hidden[:, here] = (g / (1.0 + jnp.exp(-g)) * product).astype(jnp.bfloat16)

    def share_copy(line, column, which):
        return pltpu.make_async_remote_copy(
            src_ref=part.at[line, column, which], dst_ref=parts_in.at[me, column, which],
            send_sem=rs_send, recv_sem=rs_recv.at[column, which],
            device_id={"fs": me_fs, "tp": line}, device_id_type=MESH,
        )

    def mix(line, column, which):
        here = pl.ds(pl.multiple_of((line * cols + column) * depth + which * half, 16), half)
        product = lax.dot_general(
            hidden[...], outs[2][here, :], (((1,), (1,)), ((), ())), preferred_element_type=jnp.float32
        )
        part[line, column, which] = product.astype(jnp.bfloat16)

        @pl.when(line != me)
        def _():
            share_copy(line, column, which).start()

    def mix_columns(line, which, first, cond=None):
        @pl.loop(first, cols)
        def _(c):
            if cond is None:
                mix(line, lax.rem(x + c, cols), which)
            else:
                pl.when(cond)(lambda: mix(line, lax.rem(x + c, cols), which))

    def add_up(column, which, first=False):
        ref = parts_in.at[0:tp - 1, column, which]
        pltpu.make_async_remote_copy(
            src_ref=ref, dst_ref=ref, send_sem=rs_send, recv_sem=rs_recv.at[column, which],
            device_id={"fs": me_fs, "tp": peers[0]}, device_id_type=MESH,
        ).wait_recv()
        step = 128

        @pl.loop(0, rows // step)
        def _(i):
            here = pl.ds(pl.multiple_of(i * step, step), step)
            total = part[me, column, which, here, :].astype(jnp.float32)
            for peer in peers:
                total = total + parts_in[peer, column, which, here, :].astype(jnp.float32)
            totals[column, which, here, :] = total
            powers[here, :] = total * total if first else powers[here, :] + total * total

    project(0)
    project(1)

    @pl.loop(0, lines)
    def _(line):
        mix(line, x, Q_PART)

    @pl.loop(0, lines)
    def _(line):
        mix_columns(line, P_PART, 0, jnp.logical_or(line == z, jnp.logical_not(corner)))

    inward = jnp.where(z == 0, 1, -1)
    last_p = jnp.where(z == 0, final[DOWN], final[UP])
    last_gap = (last_p - z) * inward

    def late_p(n):
        gap = n // cols + 1
        gap = jnp.where(gap < last_gap, gap, jnp.where(gap < lines - 1, gap + 1, last_gap))
        line, column = z + inward * gap, lax.rem(x + lax.rem(n, cols), cols)

        @pl.when(corner)
        def _():
            arrive(2, P_PART, line * cols + column, corner)
            mix(line, column, P_PART)

    def late_q(line):
        along_x(2, Q_PART, line)
        mix_columns(line, Q_PART, 1)

    ends, turns = (lines - 1) * cols, lines
    lead = max(0, ends - turns)

    @pl.loop(0, lead)
    def _(n):
        late_p(n)

    @pl.loop(0, ends - lead - 1)
    def _(n):
        late_p(lead + n)
        late_q(jnp.where(n < me, n, n + 1))

    add_up(x, Q_PART, True)
    for c in range(cols - 1):
        add_up(lax.rem(x + c, cols), P_PART)
    late_p(jnp.int32(ends - 1))
    late_q(me)
    add_up(lax.rem(x + cols - 1, cols), P_PART)
    for c in range(1, cols):
        add_up(lax.rem(x + c, cols), Q_PART)
    step = 128

    @pl.loop(0, rows // step)
    def _(i):
        here = pl.ds(pl.multiple_of(i * step, step), step)
        square = jnp.sum(powers[here, :], axis=1, keepdims=True)
        squares[:, here] = jnp.transpose(jnp.broadcast_to(square, (step, 128)))[0:8, :]

    def square_copy(j):
        return pltpu.make_async_remote_copy(
            src_ref=squares, dst_ref=squares_in.at[j], send_sem=sq_send, recv_sem=sq_recv.at[j],
            device_id={"fs": me_fs, "tp": peers[j]}, device_id_type=MESH,
        )

    for j in range(tp - 1):
        square_copy(j).start()
    for n in range(1, lines):
        for m in range(3):
            each = depth if m < 2 else (1 + cols) * half
            pl.when(z + 1 == n)(lambda: sent(m, UP, n * each))
            pl.when(lines - z == n)(lambda: sent(m, DOWN, n * each))
    for n in range(1, cols):
        for m in range(3):
            each = lines * depth if m < 2 else (lines + 1) * half
            pl.when(x + 1 == n)(lambda: sent(m, RIGHT, n * each))
            pl.when(cols - x == n)(lambda: sent(m, LEFT, n * each))
    token_all().wait_send()
    post_load.wait()
    ref = parts_in.at[0:tp - 1]
    pltpu.make_async_remote_copy(
        src_ref=ref, dst_ref=ref, send_sem=rs_send, recv_sem=rs_recv.at[0, 0],
        device_id={"fs": me_fs, "tp": peers[0]}, device_id_type=MESH,
    ).wait_send()
    for j in range(tp - 1):
        square_copy(j).wait_recv()
    pltpu.make_async_remote_copy(
        src_ref=squares_in, dst_ref=squares_in, send_sem=sq_send, recv_sem=sq_recv.at[0],
        device_id={"fs": me_fs, "tp": peers[0]}, device_id_type=MESH,
    ).wait_send()


def write_out(
    width, totals, squares, squares_in, gains, gate_held, up_held, down_held,
    result_out, gate_out, up_out, down_out, result, sems, last,
):
    copies = []
    for k, (ref, out) in enumerate(((gate_held, gate_out), (up_held, up_out), (down_held, down_out))):
        size = ref.shape[0] // CHUNKS
        for c in range(CHUNKS):
            here = pl.ds(c * size, size)
            copies.append(pltpu.make_async_copy(ref.at[here, :], out.at[here, :], sems.at[k, c]))
    for c in copies:
        c.start()
    rows, block = result.shape
    cols, _, _, half = totals.shape
    step = 128

    @pl.loop(0, rows // step)
    def _(i):
        here = pl.ds(pl.multiple_of(i * step, step), step)
        total = squares[:, here]
        for j in range(squares_in.shape[0]):
            total = total + squares_in[j, :, here]
        total = jnp.broadcast_to(total[0:1, :], (128, step))
        scale = lax.rsqrt(jnp.transpose(total)[:, 0:1] / width + EPS)
        for c in range(cols):
            for which in range(2):
                at = slice((2 * c + which) * half, (2 * c + which + 1) * half)
                result[here, at] = (totals[c, which, here, :] * scale * gains[0:1, at]).astype(jnp.bfloat16)

    final = pltpu.make_async_copy(result, result_out, last)
    final.start()
    for c in copies:
        c.wait()
    final.wait()


def solution(mesh):
    fs, tp = mesh.shape["fs"], mesh.shape["tp"]
    lines, cols = tp, fs // tp

    def shards(tokens, pre_gain, gate_weight, up_weight, down_weight, post_gain):
        depth, width = gate_weight.shape
        rows, block = tokens.shape
        hbm = pl.BlockSpec(memory_space=pltpu.HBM)
        vmem = pl.BlockSpec(memory_space=pltpu.VMEM)
        dma = pltpu.SemaphoreType.DMA
        half = depth // 2
        shapes = [(rows, block)] + [(fs * depth, width)] * 3
        held = pl.pallas_call(
            functools.partial(kernel, fs, tp, lines, cols),
            out_shape=(
                pltpu.VMEM((cols, 2, rows, half), jnp.float32),
                pltpu.VMEM((8, rows), jnp.float32),
                pltpu.VMEM((tp - 1, 8, rows), jnp.float32),
                pltpu.VMEM((1, block), jnp.float32),
            ) + tuple(pltpu.VMEM(s, jnp.bfloat16) for s in shapes[1:]),
            in_specs=[hbm] * 6,
            out_specs=(vmem,) * 7,
            scratch_shapes=[
                pltpu.VMEM((3, depth, width), jnp.float32),
                pltpu.VMEM((1, depth), jnp.float32),
                pltpu.VMEM((depth, 128), jnp.float32),
                pltpu.VMEM((tp, rows, block), jnp.bfloat16),
                pltpu.VMEM((rows, tp * block), jnp.bfloat16),
                pltpu.VMEM((rows, width), jnp.float32),
                pltpu.VMEM((rows, width), jnp.bfloat16),
                pltpu.VMEM((tp, cols, 2, rows, half), jnp.bfloat16),
                pltpu.VMEM((tp, cols, 2, rows, half), jnp.bfloat16),
                pltpu.VMEM((rows, half), jnp.float32),
                dma((3, 4)), dma((2, fs)), dma((2, fs)), dma((3,)), dma((2,)), dma, dma, dma,
                dma, dma((cols, 2)), dma, dma((tp - 1,)),
            ],
            compiler_params=pltpu.CompilerParams(collective_id=0, has_side_effects=True, vmem_limit_bytes=42 * 1024 * 1024),
        )(tokens, pre_gain[None, :], gate_weight, up_weight, down_weight, post_gain[None, :])
        return tuple(pl.pallas_call(
            functools.partial(write_out, tp * block),
            out_shape=tuple(jax.ShapeDtypeStruct(s, jnp.bfloat16) for s in shapes),
            in_specs=[vmem] * 7,
            out_specs=(hbm,) * 4,
            scratch_shapes=[pltpu.VMEM((rows, block), jnp.bfloat16), dma((3, CHUNKS)), dma],
            compiler_params=pltpu.CompilerParams(vmem_limit_bytes=2 * 1024 * 1024),
        )(*held))

    return jax.shard_map(
        shards,
        mesh=mesh,
        in_specs=(P("fs", "tp"), P("fs"), P("fs", "tp"), P("fs", "tp"), P("fs", "tp"), P("tp")),
        out_specs=(P("fs", "tp"), P(None, "tp"), P(None, "tp"), P(None, "tp")),
        check_vma=False,
    )
```

time: 206 us -> 198 us (0.961)
  Pallas kernels: 205 us -> 198 us
    pallas_call x1, Pallas kernels: 198 us -> 191 us  [shards(): pl.pallas_call(functools.partial(kernel, fs, tp, lines, cols), out_shape=...]
where the time goes in v1:
time: 198 us
  Pallas kernels  198 us (100%)
    pallas_call x1, Pallas kernels, shards(): pl.pallas_call(functools.partial(kernel, fs, tp, lines, cols), out_shape=...  191 us
    pallas_call x1, Pallas kernels, shards(): pl.pallas_call(functools.partial(write_out, tp * block), out_shape=tuple(...  6.72 us

profile of v1, /device:TPU:0, one launch (start us, length us, event | category | flops | bytes accessed | tf_op | source)
XLA Modules:
  0.0 198.2 jit_solution(8388344026271476111)
XLA Ops:
  0.6 190.8 %shard_map.93 = (f32[2,2,512,128]{3,2,1,0:T(8,128)S(1)}, f32[8,512]{1,0:T(8,128)S(1)}, f32[3,8,512]{2,1,0:T(8,128)S(1)}, f32[1,512]{1,0:T(1,128)S(1)}, bf16[2048...) custom-call(bf16[512,512]{1,0:T(8,128)(2,1)} %tokens.1, f32[1,256]{1,0:T(1,128)} %bitcast.3, ...), custom_call_target="tpu_custom_call" | custom-call | tf_op jit(solution)/shard_map/pallas_call | solution.py:424
  191.5 6.7 %shard_map.94 = (bf16[512,512]{1,0:T(8,128)(2,1)}, bf16[2048,1536]{1,0:T(8,128)(2,1)}, bf16[2048,1536]{1,0:T(8,128)(2,1)}, bf16[2048,1536]{1,0:T(8,128)(2,1)}) custom-call(f32[2,2,512,128]{3,2,1,0:T(8,128)S(1)} %get-tuple-element.11.totals, f32[8,512]{1,0:T(8,128)S(1)} %get-tuple-element.12.squares, f32[3,8,512]{2,1,0:T(8,128)S(1)} %get-tuple-element.13.squares_in, ...), custom_call_target="tpu_custom_call" | custom-call | tf_op jit(solution)/shard_map/pallas_call | solution.py:450

commit v2 on v1

--- a/solution.py
+++ b/solution.py
@@ -84,21 +84,21 @@
     gain_load = pltpu.make_async_copy(pre_gain, gains_row, gain_sem.at[0])
     gain_load.start()
     size = depth // CHUNKS
-    for m in range(3):
-        for c in range(CHUNKS):
-            here = pl.ds(c * size, size)
-            pltpu.make_async_copy(weights[m].at[here, :], staged.at[m, here, :], stage_sem.at[m]).start()
+
+    def load(m, c):
+        here = pl.ds(c * size, size)
+        sem = stage_sem.at[c] if m == 0 else stage_sem.at[CHUNKS + m - 1]
+        return pltpu.make_async_copy(weights[m].at[here, :], staged.at[m, here, :], sem)
+
+    for c in range(CHUNKS):
+        load(0, c).start()
     own_tokens = pltpu.make_async_copy(tokens, whole.at[me], tok_own)
-    own_tokens.start()
     post_load = pltpu.make_async_copy(post_gain, gains_out, gain_sem.at[1])
-    post_load.start()
     gain_load.wait()
     gains_in[...] = jnp.transpose(jnp.broadcast_to(gains_row[0:1, :], (128, depth)))
 
-    def cast(m):
-        pltpu.make_async_copy(weights[m], staged.at[m], stage_sem.at[m]).wait()
-
-        @pl.loop(0, depth // 16)
+    def cast(m, start, size):
+        @pl.loop(start // 16, (start + size) // 16)
         def _(i):
             here = pl.ds(pl.multiple_of(i * 16, 16), 16)
             v = staged[m, here, :]
@@ -106,6 +106,10 @@
                 v = gains_in[here, 0:1] * v
             outs[m][pl.ds(pl.multiple_of(me_fs * depth + i * 16, 16), 16), :] = v.astype(jnp.bfloat16)
 
+    def cast_all(m):
+        pltpu.make_async_copy(weights[m], staged.at[m], stage_sem.at[CHUNKS + m - 1]).wait()
+        cast(m, 0, depth)
+
     def token_copy(j):
         return pltpu.make_async_remote_copy(
             src_ref=tokens, dst_ref=whole.at[me], send_sem=tok_send, recv_sem=tok_recv,
@@ -119,16 +123,31 @@
             device_id={"fs": me_fs, "tp": peers[0]}, device_id_type=MESH,
         )
 
-    cast(0)
-    pl.semaphore_wait(barrier, tp - 1 + sum(there.astype(jnp.int32) for there, _ in sides.values()))
-    for side in sides:
-        send(0, Q_PART, me_fs, side)
+    for c in range(CHUNKS):
+        load(0, c).wait()
+        cast(0, c * size, size)
+        if c == 0:
+            for m in (1, 2):
+                for k in range(CHUNKS):
+                    load(m, k).start()
+            own_tokens.start()
+            post_load.start()
+            pl.semaphore_wait(barrier, tp - 1 + sum(there.astype(jnp.int32) for there, _ in sides.values()))
+        ref = gate_out.at[pl.ds(pl.multiple_of(me_fs * depth + c * size, 16), size), :]
+        for side, (there, target) in sides.items():
+            @pl.when(there)
+            def _():
+                pltpu.make_async_remote_copy(
+                    src_ref=ref, dst_ref=ref, send_sem=send_sem.at[0, side], recv_sem=recv_sem.at[0, me_fs],
+                    device_id={"fs": target, "tp": me}, device_id_type=MESH,
+                ).start()
+
     for j in range(tp - 1):
         token_copy(j).start()
-    cast(1)
+    cast_all(1)
     for side in sides:
         send(1, Q_PART, me_fs, side)
-    cast(2)
+    cast_all(2)
     for side in (RIGHT, LEFT):
         send(2, P_PART, me_fs, side)
 
@@ -442,7 +461,7 @@
                 pltpu.VMEM((tp, cols, 2, rows, half), jnp.bfloat16),
                 pltpu.VMEM((tp, cols, 2, rows, half), jnp.bfloat16),
                 pltpu.VMEM((rows, half), jnp.float32),
-                dma((3, 4)), dma((2, fs)), dma((2, fs)), dma((3,)), dma((2,)), dma, dma, dma,
+                dma((3, 4)), dma((2, fs)), dma((2, fs)), dma((CHUNKS + 2,)), dma((2,)), dma, dma, dma,
                 dma, dma((cols, 2)), dma, dma((tp - 1,)),
             ],
             compiler_params=pltpu.CompilerParams(collective_id=0, has_side_effects=True, vmem_limit_bytes=42 * 1024 * 1024),

time: 198 us -> 196 us (0.990)
  Pallas kernels: 198 us -> 196 us
where the time goes in v2:
time: 196 us
  Pallas kernels  196 us (100%)
    pallas_call x1, Pallas kernels, shards(): pl.pallas_call(functools.partial(kernel, fs, tp, lines, cols), out_shape=...  189 us
    pallas_call x1, Pallas kernels, shards(): pl.pallas_call(functools.partial(write_out, tp * block), out_shape=tuple(...  6.72 us

profile of v2, /device:TPU:0, one launch (start us, length us, event | category | flops | bytes accessed | tf_op | source)
XLA Modules:
  0.0 196.3 jit_solution(150948308213138533)
XLA Ops:
  0.6 189.0 %shard_map.93 = (f32[2,2,512,128]{3,2,1,0:T(8,128)S(1)}, f32[8,512]{1,0:T(8,128)S(1)}, f32[3,8,512]{2,1,0:T(8,128)S(1)}, f32[1,512]{1,0:T(1,128)S(1)}, bf16[2048...) custom-call(bf16[512,512]{1,0:T(8,128)(2,1)} %tokens.1, f32[1,256]{1,0:T(1,128)} %bitcast.3, ...), custom_call_target="tpu_custom_call" | custom-call | tf_op jit(solution)/shard_map/pallas_call | solution.py:443
  189.6 6.7 %shard_map.94 = (bf16[512,512]{1,0:T(8,128)(2,1)}, bf16[2048,1536]{1,0:T(8,128)(2,1)}, bf16[2048,1536]{1,0:T(8,128)(2,1)}, bf16[2048,1536]{1,0:T(8,128)(2,1)}) custom-call(f32[2,2,512,128]{3,2,1,0:T(8,128)S(1)} %get-tuple-element.11.totals, f32[8,512]{1,0:T(8,128)S(1)} %get-tuple-element.12.squares, f32[3,8,512]{2,1,0:T(8,128)S(1)} %get-tuple-element.13.squares_in, ...), custom_call_target="tpu_custom_call" | custom-call | tf_op jit(solution)/shard_map/pallas_call | solution.py:469
